TPU v7x, 128 devices: a whole 4x4x4 slice. The times are simulated.
128 devices in a mesh: fs: 16 (over z, y), tp: 8 (over x, core).
Axes of the slice: x: 4, y: 4, z: 4, core: 2. Of those that a mesh axis runs over, the one named last changes fastest.
Arguments:
- tokens: bfloat16 [16384, 2048], P(('fs', 'tp')), may hold values from -6 to 6
- norm_gain: float32 [2048], replicated, may hold values from 0.1 to 1.9
- up_weight: float32 [2048, 8192], P('fs', 'tp'), may hold values from -0.125 to 0.125
- down_weight: float32 [8192, 2048], P('tp', 'fs'), may hold values from -0.0625 to 0.0625
Outputs:
- mlp_out: bfloat16 [16384, 2048], P(('fs', 'tp'))
All inputs are finite; a program needn't handle non-finite values.
Results may differ from a plain program's by a relative error of at most 0.0017.
Values may be sent and summed in bfloat16 or wider, within the bound.
A program may use at most 64 MiB of HBM per device.

v0:
```python
import jax
import jax.numpy as jnp
from jax import lax
from jax.sharding import PartitionSpec as P

epsilon = 1e-06


def taken_in(slab, axis, dim, step, start):

    def gathered(part):
        return lax.all_gather(part, axis, axis=dim, tiled=True)

    return step(start, jax.tree.map(gathered, slab), jnp.int32(0))


def on_whole(shard, axis, dim, work):
    return work(lax.all_gather(shard, axis, axis=dim, tiled=True), jnp.int32(0))


def shards(tokens, norm_gain, up_weight, down_weight):
    values = tokens.astype(jnp.float32)
    scale = lax.rsqrt(jnp.mean(values * values, axis=-1, keepdims=True) + epsilon)
    normed = (values * scale * norm_gain).astype(jnp.bfloat16)
    grouped = lax.all_gather(normed, "tp", axis=0, tiled=True)
    empty = jnp.zeros((grouped.shape[0], up_weight.shape[1]), jnp.float32)

    def add_rows(total, piece, start):
        columns = lax.dynamic_slice_in_dim(grouped, start, piece.shape[0], 1)
        return total + jnp.dot(
            columns, piece.astype(jnp.bfloat16), preferred_element_type=jnp.float32
        )

    pre = taken_in(up_weight.astype(jnp.bfloat16), "fs", 0, add_rows, empty)
    hidden = jnp.square(jax.nn.relu(pre)).astype(jnp.bfloat16)

    def project(piece, start):
        return jnp.dot(hidden, piece.astype(jnp.bfloat16), preferred_element_type=jnp.float32)

    terms = on_whole(down_weight.astype(jnp.bfloat16), "fs", 1, project)
    summed = lax.psum_scatter(terms, "tp", scatter_dimension=0, tiled=True)
    return summed.astype(jnp.bfloat16)


def solution(mesh):
    placed = (P(("fs", "tp"), None), P(), P("fs", "tp"), P("tp", "fs"))
    return jax.shard_map(
        shards, mesh=mesh, in_specs=placed, out_specs=P(("fs", "tp"), None), check_vma=False
    )
```

profile of v0, /device:TPU:1, one launch (start us, length us, event | category | flops | bytes accessed | tf_op | source)
XLA Modules:
  0.0 232.5 jit_solution(14041995372060814346)
XLA Ops:
  6.5 0.0 all-gather.4.cloned.1.call-start
  6.5 1.2 fusion
  7.8 2.0 fusion.2
  9.8 0.0 all-gather.4.cloned.1.call-update
  9.8 0.0 all-gather.6.cloned.1.call-start
  9.9 1.8 convert_element_type.20
  11.7 0.0 all-gather.6.cloned.1.call-update
  11.7 0.0 all-gather.8.cloned.1.call-start
  11.7 1.8 convert_element_type.22
  13.5 0.0 all-gather.8.cloned.1.call-update
  13.5 0.0 reduce-scatter.2.cloned.1.call-start
  13.6 32.0 %all-gather.4.cloned.1.call-done = bf16[1024,2048]{1,0:T(8,128)(2,1)} async-done(((bf16[128,2048]{1,0:T(8,128)(2,1)}), bf16[1024,2048]{1,0:T(8,128)(2,1)}) %all-gather.4.cloned.1.call-update) | async-done | bytes 4194320 | tf_op jit(solution)/shard_map/all_gather | solution.py:25
  45.6 53.1 %all-gather.6.cloned.1.call-done = bf16[2048,1024]{1,0:T(8,128)(2,1)} async-done(((bf16[128,1024]{1,0:T(8,128)(2,1)}), bf16[2048,1024]{1,0:T(8,128)(2,1)}) %all-gather.6.cloned.1.call-update) | async-done | bytes 4194320 | tf_op jit(solution)/shard_map/all_gather | solution.py:12
  98.7 57.5 %all-gather.8.cloned.1.call-done = bf16[1024,2048]{1,0:T(8,128)(2,1)} async-done(((bf16[1024,128]{1,0:T(8,128)(2,1)}), bf16[1024,2048]{1,0:T(8,128)(2,1)}) %all-gather.8.cloned.1.call-update) | async-done | bytes 4194320 | tf_op jit(solution)/shard_map/all_gather | solution.py:18
  156.2 15.0 %fusion.3 = f32[1024,2048]{1,0:T(8,128)} fusion(bf16[1024,2048]{1,0:T(8,128)(2,1)} %all-gather.8.cloned.1.call-done, bf16[1024,2048]{1,0:T(8,128)(2,1)} %all-gather.4.cloned.1.call-done, bf16[2048,1024]{1,0:T(8,128)(2,1)} %all-gather.6.cloned.1.call-done), kind=kOutput, calls=%fused_computation.6 | convolution fusion | flops 8593080320 | bytes 20971520 | tf_op jit(solution)/shard_map/dot_general | solution.py:38
  171.2 0.0 reduce-scatter.2.cloned.1.call-update
  171.2 52.6 %reduce-scatter.2.cloned.1.call-done = f32[128,2048]{1,0:T(8,128)} async-done(((f32[1024,2048]{1,0:T(8,128)}), f32[128,2048]{1,0:T(8,128)}) %reduce-scatter.2.cloned.1.call-update) | async-done | bytes 1048592 | tf_op jit(solution)/shard_map/reduce_scatter | solution.py:41
  223.9 2.1 convert_element_type.23
  (1 shorter events, 0.0 us)
Async XLA Ops:
  6.5 39.1 %all-gather.4.cloned.1.call-start = ((), (), s32[]{:S(2)}) async-start(), calls=%async_computation.1 | async-start | bytes 4718592 | tf_op jit(solution)/shard_map/all_gather | solution.py:25
  9.8 88.9 %all-gather.6.cloned.1.call-start = ((), (), s32[]{:S(2)}) async-start(), calls=%async_computation.2 | async-start | bytes 4456448 | tf_op jit(solution)/shard_map/all_gather | solution.py:12
  11.7 144.5 %all-gather.8.cloned.1.call-start = ((), (), s32[]{:S(2)}) async-start(), calls=%async_computation.3 | async-start | bytes 4456448 | tf_op jit(solution)/shard_map/all_gather | solution.py:18
  13.5 210.4 %reduce-scatter.2.cloned.1.call-start = ((), (), s32[]{:S(2)}) async-start(), calls=%async_computation.4 | async-start | bytes 9437184 | tf_op jit(solution)/shard_map/reduce_scatter | solution.py:41
Sparse Core Ops, SparseCore 0:
  9.9 35.6 all-gather.3
  47.7 50.9 all-gather.5
  100.8 55.3 all-gather.7
  171.4 52.4 reduce-scatter.1
where the time goes:
time: 233 us
  waiting for transfers between devices  195 us (84%)
  matrix products  15 us (6%)
  between operations  13.1 us (6%)
  other arithmetic  8.9 us (4%)
    all_gather x1, waiting for transfers between devices, on_whole(): return work(lax.all_gather(shard, axis, axis=dim, tiled=True), jnp.int32(0))  57.5 us
    all_gather x1, waiting for transfers between devices, gathered(): return lax.all_gather(part, axis, axis=dim, tiled=True)  53.1 us
    reduce_scatter x1, waiting for transfers between devices, shards(): summed = lax.psum_scatter(terms, 'tp', scatter_dimension=0, tiled=True)  52.6 us
    all_gather x1, waiting for transfers between devices, shards(): grouped = lax.all_gather(normed, 'tp', axis=0, tiled=True)  32 us
    dot_general x1, matrix products, project(): jnp.dot(hidden, piece.astype(jnp.bfloat16), preferred_element_type=jnp.fl...  15 us
  transfers between devices with their start and end apart: 4, of which 4 were waited for; matrix products, arithmetic and copies ran while one was open for 2% of the time, Pallas kernels for 0%

commit v1 on v0

--- a/solution.py
+++ b/solution.py
@@ -4,6 +4,18 @@
 from jax.sharding import PartitionSpec as P
 
 epsilon = 1e-06
+
+
+def gather_by_bits(value, axis, dim):
+    ways, here, turn = (lax.axis_size(axis), lax.axis_index(axis), value.shape[dim])
+    line, have = (value, 1)
+    while have < ways:
+        line = jnp.concatenate(
+            [line, lax.ppermute(line, axis, [(d, (d - have) % ways) for d in range(ways)])],
+            axis=dim,
+        )
+        have = 2 * have
+    return jnp.roll(line, here * turn, axis=dim)
 
 
 def taken_in(slab, axis, dim, step, start):
@@ -22,7 +34,7 @@
     values = tokens.astype(jnp.float32)
     scale = lax.rsqrt(jnp.mean(values * values, axis=-1, keepdims=True) + epsilon)
     normed = (values * scale * norm_gain).astype(jnp.bfloat16)
-    grouped = lax.all_gather(normed, "tp", axis=0, tiled=True)
+    grouped = gather_by_bits(normed, "tp", 0)
     empty = jnp.zeros((grouped.shape[0], up_weight.shape[1]), jnp.float32)
 
     def add_rows(total, piece, start):

time: 233 us -> 198 us (0.85)
  waiting for transfers between devices: 195 us -> 143 us
  local copies, waits for them, and re-layouts: 0 us -> 8.68 us
  starting transfers between devices: 0.13 us -> 7.5 us
    ppermute x0 -> x3, waiting for transfers between devices: none -> 72.2 us  [gather_by_bits(): lax.ppermute(line, axis, [(d, (d - have) % ways) for d in range(ways)])]
    all_gather x1, waiting for transfers between devices: 53.1 us -> 0.01 us  [gathered(): return lax.all_gather(part, axis, axis=dim, tiled=True)]
    all_gather x1, waiting for transfers between devices: 57.5 us -> 18.1 us  [on_whole(): return work(lax.all_gather(shard, axis, axis=dim, tiled=True), jnp.int32(0))]
    all_gather x1 -> x0, waiting for transfers between devices: 32 us -> none  [shards(): grouped = lax.all_gather(normed, 'tp', axis=0, tiled=True)]
    ppermute x0 -> x3, starting transfers between devices: none -> 7.42 us  [gather_by_bits(): lax.ppermute(line, axis, [(d, (d - have) % ways) for d in range(ways)])]
    unnamed x0 -> x14, local copies, waits for them, and re-layouts: none -> 7.25 us
  transfers between devices with their start and end apart: 4 -> 6, of which waited for: 4 -> 5; matrix products, arithmetic and copies ran while one was open for 2% -> 8% of each run, Pallas kernels for 0% -> 0%
where the time goes in v1:
time: 198 us
  waiting for transfers between devices  143 us (72%)
  matrix products  15 us (8%)
  between operations  13.1 us (7%)
  other arithmetic  10.5 us (5%)
  local copies, waits for them, and re-layouts  8.68 us (4%)
  starting transfers between devices  7.5 us (4%)
    ppermute x3, waiting for transfers between devices, gather_by_bits(): lax.ppermute(line, axis, [(d, (d - have) % ways) for d in range(ways)])  72.2 us
    reduce_scatter x1, waiting for transfers between devices, shards(): summed = lax.psum_scatter(terms, 'tp', scatter_dimension=0, tiled=True)  52.6 us
    all_gather x1, waiting for transfers between devices, on_whole(): return work(lax.all_gather(shard, axis, axis=dim, tiled=True), jnp.int32(0))  18.1 us
    dot_general x1, matrix products, project(): jnp.dot(hidden, piece.astype(jnp.bfloat16), preferred_element_type=jnp.fl...  15 us
    ppermute x3, starting transfers between devices, gather_by_bits(): lax.ppermute(line, axis, [(d, (d - have) % ways) for d in range(ways)])  7.42 us
    unnamed x14, local copies, waits for them, and re-layouts  7.25 us
  transfers between devices with their start and end apart: 6, of which 5 were waited for; matrix products, arithmetic and copies ran while one was open for 8% of the time, Pallas kernels for 0%

profile of v1, /device:TPU:1, one launch (start us, length us, event | category | flops | bytes accessed | tf_op | source)
XLA Modules:
  0.0 197.9 jit_solution(9362928776961155883)
XLA Ops:
  6.5 1.8 convert_element_type.20
  8.3 0.0 all-gather.5.cloned.1.call-start
  8.4 1.8 convert_element_type.22
  10.3 1.2 fusion.8
  11.5 2.1 %constant_dynamic-update-slice_fusion.7 = (bf16[2048,2048]{1,0:T(8,128)(2,1)}, bf16[128,2048]{1,0:T(8,128)(2,1)S(1)}) fusion(f32[2048]{0:T(1024)} %param.5, f32[128]{0:T(128)S(1)} %add_rsqrt_fusion, bf16[128,2048]{1,0:T(8,128)(2,1)} %param.4), kind=kLoop, calls=%fused_computation.19 | loop fusion | flops 1048575 | bytes 1581568
  13.6 1.4 collective-permute-start
  15.0 8.1 %collective-permute-done = bf16[128,2048]{1,0:T(8,128)(2,1)S(1)} collective-permute-done((bf16[128,2048]{1,0:T(8,128)(2,1)S(1)}, bf16[128,2048]{1,0:T(8,128)(2,1)S(1)}, u32[]{:S(2)}, u32[]{:S(2)}) %collective-permute-start) | collective-permute-done | bytes 524320 | tf_op jit(solution)/shard_map/ppermute | solution.py:14
  23.0 0.1 pad_maximum_fusion.1
  23.1 3.7 %collective-permute-start.1 = (bf16[256,2048]{1,0:T(8,128)(2,1)S(1)}, bf16[256,2048]{1,0:T(8,128)(2,1)S(1)}, u32[]{:S(2)}, u32[]{:S(2)}) collective-permute-start(bf16[256,2048]{1,0:T(8,128)(2,1)S(1)} %pad_maximum_fusion.1), channel_id=1, source_target_pairs={{0,6},{1,7},{2,0},{3,1},{4,2},{5,3},{6,4},{7,5},{8,14},{9,15},{10,... | collective-permute-start | bytes 3145736 | tf_op jit(solution)/shard_map/ppermute | solution.py:14
  26.8 21.3 %collective-permute-done.1 = bf16[256,2048]{1,0:T(8,128)(2,1)S(1)} collective-permute-done((bf16[256,2048]{1,0:T(8,128)(2,1)S(1)}, bf16[256,2048]{1,0:T(8,128)(2,1)S(1)}, u32[]{:S(2)}, u32[]{:S(2)}) %collective-permute-start.1) | collective-permute-done | bytes 1048608 | tf_op jit(solution)/shard_map/ppermute | solution.py:14
  48.1 1.5 pad_maximum_fusion
  49.6 2.3 %collective-permute-start.2 = (bf16[512,2048]{1,0:T(8,128)(2,1)}, bf16[512,2048]{1,0:T(8,128)(2,1)S(1)}, u32[]{:S(2)}, u32[]{:S(2)}) collective-permute-start(bf16[512,2048]{1,0:T(8,128)(2,1)} %pad_maximum_fusion), channel_id=1, source_target_pairs={{0,4},{1,5},{2,6},{3,7},{4,0},{5,1},{6,2},{7,3},{8,12},{9,13},{10,... | collective-permute-start | bytes 6291464 | tf_op jit(solution)/shard_map/ppermute | solution.py:14
  51.9 2.0 %constant_dynamic-update-slice_fusion.6 = bf16[2048,2048]{1,0:T(8,128)(2,1)} fusion(bf16[2048,2048]{1,0:T(8,128)(2,1)} %get-tuple-element.5, bf16[128,2048]{1,0:T(8,128)(2,1)} %copy-done.2), kind=kLoop, calls=%fused_computation.18 | loop fusion | bytes 1048576
  53.9 1.0 constant_dynamic-update-slice_fusion.5
  54.9 42.9 %collective-permute-done.2 = bf16[512,2048]{1,0:T(8,128)(2,1)S(1)} collective-permute-done((bf16[512,2048]{1,0:T(8,128)(2,1)}, bf16[512,2048]{1,0:T(8,128)(2,1)S(1)}, u32[]{:S(2)}, u32[]{:S(2)}) %collective-permute-start.2) | collective-permute-done | bytes 2097184 | tf_op jit(solution)/shard_map/ppermute | solution.py:14
  97.9 1.5 constant_dynamic-update-slice_fusion.4
  99.3 0.8 constant_dynamic-update-slice_fusion.3
  100.2 0.8 constant_dynamic-update-slice_fusion.2
  101.0 1.0 constant_dynamic-update-slice_fusion.1
  102.1 1.4 constant_dynamic-update-slice_fusion
  103.5 18.1 %all-gather.5.cloned.1.call-done = bf16[1024,2048]{1,0:T(8,128)(2,1)} async-done(((bf16[1024,128]{1,0:T(8,128)(2,1)}), bf16[1024,2048]{1,0:T(8,128)(2,1)}) %all-gather.5.cloned.1.call-update) | async-done | bytes 4194320 | tf_op jit(solution)/shard_map/all_gather | solution.py:30
  121.6 15.0 %fusion.2 = f32[1024,2048]{1,0:T(8,128)} fusion(bf16[1024,2048]{1,0:T(8,128)(2,1)} %all-gather.5.cloned.1.call-done, bf16[2048,1024]{1,0:T(8,128)(2,1)} %all-gather.3.cloned.1.call-done, bf16[2048,2048]{1,0:T(8,128)(2,1)} %constant_dynamic-update-slice_fusion, s32[]{:T(128)S(6)} %select_n.14), kind=kOutput, calls=%fused_computation.3 | convolution fusion | flops 8593080320 | bytes 20971524 | tf_op jit(solution)/shard_map/dot_general | solution.py:50
  136.6 52.6 %reduce-scatter.2.cloned.1.call-done = f32[128,2048]{1,0:T(8,128)} async-done(((f32[1024,2048]{1,0:T(8,128)}), f32[128,2048]{1,0:T(8,128)}) %reduce-scatter.2.cloned.1.call-update) | async-done | bytes 1048592 | tf_op jit(solution)/shard_map/reduce_scatter | solution.py:53
  189.2 2.1 %convert_element_type.23 = bf16[128,2048]{1,0:T(8,128)(2,1)} convert(f32[128,2048]{1,0:T(8,128)} %reduce-scatter.2.cloned.1.call-done) | non-fusion elementwise | flops 262144 | bytes 1572864 | tf_op jit(solution)/shard_map/convert_element_type | solution.py:54
  (15 shorter events, 0.1 us)
Async XLA Ops:
  6.5 97.0 %all-gather.3.cloned.1.call-start = ((), (), s32[]{:S(2)}) async-start(), calls=%async_computation.1 | async-start | bytes 4456448 | tf_op jit(solution)/shard_map/all_gather | solution.py:24
  8.3 113.2 %all-gather.5.cloned.1.call-start = ((), (), s32[]{:S(2)}) async-start(), calls=%async_computation.2 | async-start | bytes 4456448 | tf_op jit(solution)/shard_map/all_gather | solution.py:30
  10.2 179.0 %reduce-scatter.2.cloned.1.call-start = ((), (), s32[]{:S(2)}) async-start(), calls=%async_computation.3 | async-start | bytes 9437184 | tf_op jit(solution)/shard_map/reduce_scatter | solution.py:53
  13.6 34.5 %copy-start = (bf16[128,2048]{1,0:T(8,128)(2,1)}, bf16[128,2048]{1,0:T(8,128)(2,1)S(1)}, u32[]{:S(2)}) copy-start(bf16[128,2048]{1,0:T(8,128)(2,1)S(1)} %get-tuple-element.6) | copy-start | bytes 1572868
  13.6 9.5 %collective-permute-start = (bf16[128,2048]{1,0:T(8,128)(2,1)S(1)}, bf16[128,2048]{1,0:T(8,128)(2,1)S(1)}, u32[]{:S(2)}, u32[]{:S(2)}) collective-permute-start(bf16[128,2048]{1,0:T(8,128)(2,1)S(1)} %get-tuple-element.6), channel_id=1, source_target_pairs={{0,7},{1,0},{2,1},{3,2},{4,3},{5,4},{6,5},{7,6},{8,15},{9,8},{10,9... | collective-permute-start | bytes 1572872 | tf_op jit(solution)/shard_map/ppermute | solution.py:14
  23.0 26.6 %copy-start.2 = (bf16[128,2048]{1,0:T(8,128)(2,1)}, bf16[128,2048]{1,0:T(8,128)(2,1)S(1)}, u32[]{:S(2)}) copy-start(bf16[128,2048]{1,0:T(8,128)(2,1)S(1)} %collective-permute-done) | copy-start | bytes 1572868
  23.1 25.0 %collective-permute-start.1 = (bf16[256,2048]{1,0:T(8,128)(2,1)S(1)}, bf16[256,2048]{1,0:T(8,128)(2,1)S(1)}, u32[]{:S(2)}, u32[]{:S(2)}) collective-permute-start(bf16[256,2048]{1,0:T(8,128)(2,1)S(1)} %pad_maximum_fusion.1), channel_id=1, source_target_pairs={{0,6},{1,7},{2,0},{3,1},{4,2},{5,3},{6,4},{7,5},{8,14},{9,15},{10,... | collective-permute-start | bytes 3145736 | tf_op jit(solution)/shard_map/ppermute | solution.py:14
  49.6 48.3 %collective-permute-start.2 = (bf16[512,2048]{1,0:T(8,128)(2,1)}, bf16[512,2048]{1,0:T(8,128)(2,1)S(1)}, u32[]{:S(2)}, u32[]{:S(2)}) collective-permute-start(bf16[512,2048]{1,0:T(8,128)(2,1)} %pad_maximum_fusion), channel_id=1, source_target_pairs={{0,4},{1,5},{2,6},{3,7},{4,0},{5,1},{6,2},{7,3},{8,12},{9,13},{10,... | collective-permute-start | bytes 6291464 | tf_op jit(solution)/shard_map/ppermute | solution.py:14
  51.9 47.4 %copy-start.1 = (bf16[128,2048]{1,0:T(8,128)(2,1)S(1)}, bf16[128,2048]{1,0:T(8,128)(2,1)}, u32[]{:S(2)}) copy-start(bf16[128,2048]{1,0:T(8,128)(2,1)} %copy-done) | copy-start | bytes 1572868
  51.9 48.3 %copy-start.3 = (bf16[128,2048]{1,0:T(8,128)(2,1)S(1)}, bf16[128,2048]{1,0:T(8,128)(2,1)}, u32[]{:S(2)}) copy-start(bf16[128,2048]{1,0:T(8,128)(2,1)} %copy-done.2) | copy-start | bytes 1572868
Sparse Core Ops, SparseCore 0:
  9.5 54.5 all-gather.2
  66.2 55.3 all-gather.4
  136.7 52.4 reduce-scatter.1
